TPU v7x, 32 devices: a whole 2x2x4 slice. The times are simulated.
32 devices in a mesh: grp: 2 (over y), fs: 4 (over z), tp: 4 (over x, core).
Axes of the slice: x: 2, y: 2, z: 4, core: 2. Of those that a mesh axis runs over, the one named last changes fastest.
Arguments:
- tokens: bfloat16 [4096, 2048], P(('grp', 'fs')), parts along dimension 0, may hold values from -6 to 6
- norm_in: bfloat16 [2048], replicated, may hold values from 0.099609375 to 1.8984375
- w_value: bfloat16 [2048, 2048], P('fs', 'tp'), may hold values from -0.125 to 0.125
- w_gate: bfloat16 [2048, 2048], P('fs', 'tp'), may hold values from -0.125 to 0.125
- conv_kernel: float32 [31, 2048], replicated, as said below
- ln_gain: bfloat16 [2048], replicated, may hold values from 0.099609375 to 1.8984375
- ln_shift: bfloat16 [2048], replicated, may hold values from -3 to 3
- w_out: bfloat16 [2048, 2048], P('tp', 'fs'), may hold values from -0.125 to 0.125
- norm_mlp: bfloat16 [2048], replicated, may hold values from 0.099609375 to 1.8984375
- w_up: bfloat16 [2048, 8192], P('fs', 'tp'), may hold values from -0.125 to 0.125
- w_down: bfloat16 [8192, 2048], P('tp', 'fs'), may hold values from -0.0625 to 0.0625
Outputs:
- layer_out: bfloat16 [4096, 2048], P(('grp', 'fs', 'tp')), parts along dimension 0
There are 2 independent parts, one for each index of `grp`. A program takes and returns all parts, laid end to end along the dimension named above; an argument that names none is the same for every part. Nothing has to cross between parts.
Inputs may be any that keep to these rules, and one draw needn't show every extreme that they name: `conv_kernel`: a depthwise kernel.
All inputs are finite; a program needn't handle non-finite values.
Results may differ from a plain program's by a relative error of at most 0.018.
Values may be sent and summed in bfloat16 or wider, within the bound.
A program may use at most 64 MiB of HBM per device.

v0:
```python
import jax
import jax.numpy as jnp
from jax import lax
from jax.sharding import PartitionSpec as P

D = 2048
KERNEL = 31


def rms_scale(values, gain):
    as_float = values.astype(jnp.float32)
    scaled = as_float * lax.rsqrt(jnp.mean(as_float * as_float, axis=-1, keepdims=True) + 1e-06)
    return scaled * gain.astype(jnp.float32)


def shards(
    tokens, norm_in, w_value, w_gate, conv_kernel, ln_gain, ln_shift, w_out, norm_mlp, w_up, w_down
):
    seq_len = tokens.shape[0]
    col_width = w_value.shape[1]
    offset = lax.axis_index("tp") * col_width
    row_share = seq_len // lax.axis_size("tp")
    own_start = lax.axis_index("tp") * row_share
    normed_in = rms_scale(tokens, norm_in).astype(jnp.bfloat16)
    columns = normed_in
    values_f = jnp.dot(
        columns,
        lax.all_gather(w_value, "fs", axis=0, tiled=True),
        preferred_element_type=jnp.float32,
    )
    gate_act = jnp.dot(
        columns,
        lax.all_gather(w_gate, "fs", axis=0, tiled=True),
        preferred_element_type=jnp.float32,
    )
    gated = values_f * jax.nn.sigmoid(gate_act)
    kernel = lax.dynamic_slice_in_dim(conv_kernel, offset, col_width, 1)
    padded = jnp.pad(gated, ((KERNEL - 1, 0), (0, 0)))
    convolved = jnp.zeros_like(gated)
    for tap_index in range(KERNEL):
        convolved = convolved + kernel[tap_index][None, :] * padded[tap_index : tap_index + seq_len]
    stats = lax.psum((jnp.sum(convolved, axis=1), jnp.sum(convolved * convolved, axis=1)), "tp")
    chan_mean = (stats[0] / D)[:, None]
    chan_msq = (stats[1] / D)[:, None]
    variance = chan_msq - chan_mean * chan_mean
    gain_part = lax.dynamic_slice_in_dim(ln_gain, offset, col_width, 0).astype(jnp.float32)
    shift_part = lax.dynamic_slice_in_dim(ln_shift, offset, col_width, 0).astype(jnp.float32)
    normed = (convolved - chan_mean) * lax.rsqrt(variance + 1e-05) * gain_part + shift_part
    activated = jax.nn.silu(normed).astype(jnp.bfloat16)
    partial_value = jnp.dot(
        activated,
        lax.all_gather(w_out, "fs", axis=1, tiled=True),
        preferred_element_type=jnp.float32,
    )
    mixed = lax.psum(partial_value.astype(jnp.bfloat16), "tp").astype(jnp.float32)
    residual = tokens.astype(jnp.float32) + mixed
    normed_mlp = rms_scale(residual, norm_mlp).astype(jnp.bfloat16)
    residual_own = lax.dynamic_slice_in_dim(residual, own_start, row_share, 0)
    columns = normed_mlp
    up_act = jnp.dot(
        columns, lax.all_gather(w_up, "fs", axis=0, tiled=True), preferred_element_type=jnp.float32
    )
    hidden = jnp.square(jax.nn.relu(up_act)).astype(jnp.bfloat16)
    whole_down = lax.all_gather(w_down, "fs", axis=1, tiled=True)
    mlp_own = lax.psum_scatter(
        jnp.dot(hidden, whole_down, preferred_element_type=jnp.float32).astype(jnp.bfloat16),
        "tp",
        scatter_dimension=0,
        tiled=True,
    ).astype(jnp.float32)
    return (residual_own + mlp_own).astype(jnp.bfloat16)


def solution(mesh):
    in_specs = (
        P(("grp", "fs"), None),
        P(),
        P("fs", "tp"),
        P("fs", "tp"),
        P(),
        P(),
        P(),
        P("tp", "fs"),
        P(),
        P("fs", "tp"),
        P("tp", "fs"),
    )
    out_specs = P(("grp", "fs", "tp"), None)
    return jax.shard_map(shards, mesh=mesh, in_specs=in_specs, out_specs=out_specs, check_vma=False)
```

profile of v0, /device:TPU:0, one launch (start us, length us, event | category | flops | bytes accessed | tf_op | source)
XLA Modules:
  0.0 559.9 jit_solution(14983291080787817863)
XLA Ops:
  6.5 0.0 copy-start
  6.5 0.0 all-gather.8.cloned.1.call-start
  6.5 0.7 all-gather.8.cloned.1.call-update
  7.3 0.0 all-gather.6.cloned.1.call-start
  7.3 0.7 all-gather.6.cloned.1.call-update
  8.0 0.0 all-gather.10.cloned.1.call-start
  8.1 0.7 all-gather.10.cloned.1.call-update
  8.7 0.0 all-reduce.4.cloned.1.call-start
  8.8 0.7 convert_element_type.46
  9.5 0.8 dynamic-slice_convert_fusion
  10.3 1.1 fusion.50
  11.4 1.4 constant_dynamic-slice_fusion
  12.8 2.1 fusion
  14.8 42.5 %all-gather.8.cloned.1.call-done = bf16[2048,512]{1,0:T(8,128)(2,1)} async-done(((bf16[512,512]{1,0:T(8,128)(2,1)}), bf16[2048,512]{1,0:T(8,128)(2,1)}) %all-gather.8.cloned.1.call-update) | async-done | bytes 2097168 | tf_op jit(solution)/shard_map/all_gather | solution.py:33
  57.3 0.0 copy-done
  57.3 3.0 fusion.7
  60.4 43.0 %all-gather.6.cloned.1.call-done = bf16[2048,512]{1,0:T(8,128)(2,1)} async-done(((bf16[512,512]{1,0:T(8,128)(2,1)}), bf16[2048,512]{1,0:T(8,128)(2,1)}) %all-gather.6.cloned.1.call-update) | async-done | bytes 2097168 | tf_op jit(solution)/shard_map/all_gather | solution.py:28
  103.4 2.9 convolution_multiply_fusion
  106.3 5.0 fusion.49
  111.3 6.8 %all-reduce.1 = (f32[512]{0:T(512)S(1)}, f32[512]{0:T(512)S(1)}) all-reduce(f32[512]{0:T(512)S(1)} %get-tuple-element.6, f32[512]{0:T(512)S(1)} %get-tuple-element.5), channel_id=1, replica_groups=mesh['grp'=2,'fs'=4,'tp'=4] {'tp'}, use_global_device_ids=true, to_apply=%region_4.5 | all-reduce | flops 1024 | bytes 8192 | tf_op jit(solution)/shard_map/psum | solution.py:42
  118.1 31.4 %all-gather.10.cloned.1.call-done = bf16[512,2048]{1,0:T(8,128)(2,1)} async-done(((bf16[512,512]{1,0:T(8,128)(2,1)}), bf16[512,2048]{1,0:T(8,128)(2,1)}) %all-gather.10.cloned.1.call-update) | async-done | bytes 2097168 | tf_op jit(solution)/shard_map/all_gather | solution.py:52
  149.4 4.4 convolution_convert_fusion.1
  153.9 0.0 all-reduce.4.cloned.1.call-update
  153.9 0.0 copy-start.1
  153.9 0.0 all-gather.12.cloned.1.call-start
  153.9 0.5 all-gather.12.cloned.1.call-update
  154.5 0.0 all-gather.14.cloned.1.call-start
  154.5 0.5 all-gather.14.cloned.1.call-update
  155.1 0.2 reduce-scatter.2.cloned.1.call-start
  155.3 0.0 copy-done.1
  155.3 48.9 %all-reduce.4.cloned.1.call-done = bf16[512,2048]{1,0:T(8,128)(2,1)} async-done(((bf16[512,2048]{1,0:T(8,128)(2,1)}), bf16[512,2048]{1,0:T(8,128)(2,1)}) %all-reduce.4.cloned.1.call-update) | async-done | bytes 2097168 | tf_op jit(solution)/shard_map/psum | solution.py:55
  204.2 4.2 convert_add_fusion
  208.4 146.9 %all-gather.12.cloned.1.call-done = bf16[2048,2048]{1,0:T(8,128)(2,1)} async-done(((bf16[512,2048]{1,0:T(8,128)(2,1)}), bf16[2048,2048]{1,0:T(8,128)(2,1)}) %all-gather.12.cloned.1.call-update) | async-done | bytes 8388624 | tf_op jit(solution)/shard_map/all_gather | solution.py:61
  355.4 149.3 %all-gather.14.cloned.1.call-done = bf16[2048,2048]{1,0:T(8,128)(2,1)} async-done(((bf16[2048,512]{1,0:T(8,128)(2,1)}), bf16[2048,2048]{1,0:T(8,128)(2,1)}) %all-gather.14.cloned.1.call-update) | async-done | bytes 8388624 | tf_op jit(solution)/shard_map/all_gather | solution.py:64
  504.6 16.6 %convolution_convert_fusion = bf16[512,2048]{1,0:T(8,128)(2,1)} fusion(bf16[2048,2048]{1,0:T(8,128)(2,1)} %all-gather.14.cloned.1.call-done, bf16[2048,2048]{1,0:T(8,128)(2,1)} %all-gather.12.cloned.1.call-done, f32[2048]{0:T(1024)S(1)} %convert_element_type.53, f32[512]{0:T(512)S(1)} %add_rsqrt_fusion, bf16[512,2048]{1,0:T(8,128)(2,1)S(1)} %copy-done, ...), kind=kOutput, calls=%fused_computation.9 | convolution fusion | flops 8600420352 | bytes 23078912 | tf_op jit(solution)/shard_map/dot_general | solution.py:66
  521.2 0.0 reduce-scatter.2.cloned.1.call-update
  521.2 29.5 %reduce-scatter.2.cloned.1.call-done = bf16[128,2048]{1,0:T(8,128)(2,1)} async-done(((bf16[512,2048]{1,0:T(8,128)(2,1)}), bf16[128,2048]{1,0:T(8,128)(2,1)}) %reduce-scatter.2.cloned.1.call-update) | async-done | bytes 524304 | tf_op jit(solution)/shard_map/reduce_scatter | solution.py:65
  550.8 2.3 add_convert_fusion
  (4 shorter events, 0.0 us)
Async XLA Ops:
  6.5 50.8 %copy-start = (bf16[512,2048]{1,0:T(8,128)(2,1)S(1)}, bf16[512,2048]{1,0:T(8,128)(2,1)}, u32[]{:S(2)}) copy-start(bf16[512,2048]{1,0:T(8,128)(2,1)} %param.11) | copy-start | bytes 6291460
  6.5 50.8 %all-gather.8.cloned.1.call-start = ((), (), s32[]{:S(2)}) async-start(), calls=%async_computation.2 | async-start | bytes 2621440 | tf_op jit(solution)/shard_map/all_gather | solution.py:33
  7.3 96.1 %all-gather.6.cloned.1.call-start = ((), (), s32[]{:S(2)}) async-start(), calls=%async_computation.1 | async-start | bytes 2621440 | tf_op jit(solution)/shard_map/all_gather | solution.py:28
  8.0 141.4 %all-gather.10.cloned.1.call-start = ((), (), s32[]{:S(2)}) async-start(), calls=%async_computation.3 | async-start | bytes 2621440 | tf_op jit(solution)/shard_map/all_gather | solution.py:52
  8.7 195.5 %all-reduce.4.cloned.1.call-start = ((), (), s32[]{:S(2)}) async-start(), calls=%async_computation.4 | async-start | bytes 4194304 | tf_op jit(solution)/shard_map/psum | solution.py:55
  153.9 1.4 copy-start.1
  153.9 201.5 %all-gather.12.cloned.1.call-start = ((), (), s32[]{:S(2)}) async-start(), calls=%async_computation.5 | async-start | bytes 10485760 | tf_op jit(solution)/shard_map/all_gather | solution.py:61
  154.5 350.1 %all-gather.14.cloned.1.call-start = ((), (), s32[]{:S(2)}) async-start(), calls=%async_computation.6 | async-start | bytes 10485760 | tf_op jit(solution)/shard_map/all_gather | solution.py:64
  155.1 395.7 %reduce-scatter.2.cloned.1.call-start = ((), (), s32[]{:S(2)}) async-start(), calls=%async_computation.7 | async-start | bytes 2621440 | tf_op jit(solution)/shard_map/reduce_scatter | solution.py:65
Sparse Core Ops, SparseCore 0:
  8.9 48.3 all-gather.7
  58.9 44.4 all-gather.5
  105.0 44.4 all-gather.9
  154.0 50.1 all-reduce.3
  205.6 149.6 all-gather.11
  356.8 147.7 all-gather.13
  521.4 29.3 reduce-scatter.1
where the time goes:
time: 560 us
  waiting for transfers between devices  495 us (88%)
  matrix products  26.9 us (5%)
  other arithmetic  15 us (3%)
  between operations  13.6 us (2%)
  blocking collectives  6.79 us (1%)
    all_gather x1, waiting for transfers between devices, shards(): whole_down = lax.all_gather(w_down, 'fs', axis=1, tiled=True)  149 us
    all_gather x1, waiting for transfers between devices, shards(): lax.all_gather(w_up, 'fs', axis=0, tiled=True)  147 us
    psum x1, waiting for transfers between devices, shards(): lax.psum(partial_value.astype(jnp.bfloat16), 'tp').astype(jnp.float32)  48.9 us
    all_gather x1, waiting for transfers between devices, shards(): lax.all_gather(w_value, 'fs', axis=0, tiled=True)  43 us
    all_gather x1, waiting for transfers between devices, shards(): lax.all_gather(w_gate, 'fs', axis=0, tiled=True)  42.5 us
    all_gather x1, waiting for transfers between devices, shards(): lax.all_gather(w_out, 'fs', axis=1, tiled=True)  31.4 us
    reduce_scatter x1, waiting for transfers between devices, shards(): lax.psum_scatter(jnp.dot(hidden, whole_down, preferred_element_type=jnp.f...  29.5 us
    dot_general x1, matrix products, shards(): jnp.dot(hidden, whole_down, preferred_element_type=jnp.float32)  16.6 us
  transfers between devices with their start and end apart: 7, of which 7 were waited for; matrix products, arithmetic and copies ran while one was open for 4% of the time, Pallas kernels for 0%

commit v1 on v0

v1 whole, which is shorter than its diff:
```python
import functools

import jax
import jax.numpy as jnp
from jax import lax
from jax.experimental import pallas as pl
from jax.experimental.pallas import tpu as pltpu
from jax.sharding import PartitionSpec as P

MESH = pl.DeviceIdType.MESH
PIECES = 4
AHEAD = 3
PAD = 32


def rms_rows(x, gain):
    return x * lax.rsqrt(jnp.mean(x * x, axis=-1, keepdims=True) + 1e-06) * gain


def kernel(
    F, T,
    tok, norm_in, conv_k, ln_gain, ln_shift, norm_mlp, wv, wg, wo, wu, wd,
    out,
    normed, gv, gg, go, gu, gd, gated, conv, act, part, rs, resid, nm, hidden, fin, rs2,
    st_own, st_recv, nm_own,
    local_sem, zsend_r, zsend_l, zrecv_r, zrecv_l, ysend_r, ysend_l, yrecv_r, yrecv_l,
    st_send, st_rsem, rs_send, rs_rsem, ag_send, ag_rsem, fs_send, fs_rsem,
):
    g = lax.axis_index("grp")
    z = lax.axis_index("fs")
    t = lax.axis_index("tp")
    S, D = tok.shape
    R, C = wv.shape
    H = wu.shape[1]
    N = wo.shape[1]
    taps = conv_k.shape[0]
    rows = S // T
    R2, C2, H2 = R // 2, C // 2, H // 2
    HB, HC = H // PIECES, H2 // PIECES
    other = 1 - g
    n_chunks = 3 + 2 * PIECES
    first_down = 3 + PIECES

    def mult(i, k):
        return pl.multiple_of(i, k)

    def own(c, h):
        if c < 3:
            ref, size = ((wv, R2), (wg, R2), (wo, C2))[c]
            return ref.at[pl.ds(mult(h * size, size), size), :]
        if c < first_down:
            return wu.at[pl.ds(mult(h * R2, R2), R2), pl.ds((c - 3) * HB, HB)]
        return wd.at[pl.ds(mult(h * H2 + (c - first_down) * HC, HC), HC), :]

    def slot(c, src, h):
        if c < 2:
            return (gv, gg)[c].at[pl.ds(mult(src * R + h * R2, R2), R2), :]
        if c == 2:
            return go.at[src, pl.ds(mult(h * C2, C2), C2), :]
        if c < first_down:
            return gu.at[c - 3, pl.ds(mult(src * R + h * R2, R2), R2), :]
        return gd.at[src, pl.ds(mult(h * H2 + (c - first_down) * HC, HC), HC), :]

    def remote(src_ref, dst_ref, send, recv, device):
        return pltpu.make_async_remote_copy(
            src_ref=src_ref, dst_ref=dst_ref, send_sem=send, recv_sem=recv,
            device_id=device, device_id_type=MESH,
        )

    peers = [lax.rem(t + i, T) for i in range(T)]
    sources = [lax.rem(t - i + T, T) for i in range(T)]

    barrier = pltpu.get_barrier_semaphore()

    def greet(device):
        pl.semaphore_signal(barrier, inc=1, device_id=device, device_id_type=MESH)

    greet((other, z, t))
    for i in range(1, T):
        greet((g, z, peers[i]))

    @pl.when(z > 0)
    def _():
        greet((g, z - 1, t))

    @pl.when(z < F - 1)
    def _():
        greet((g, z + 1, t))

    ends = lax.div(z + F - 1, F) + lax.div(2 * F - 2 - z, F)
    pl.semaphore_wait(barrier, T + ends)

    ys, yr = (ysend_r, ysend_l), (yrecv_r, yrecv_l)

    def own_right(c):
        return remote(own(c, g), slot(c, z, g), zsend_r.at[c, 0], zrecv_r.at[c, 1], (g, z + 1, t))

    def own_left(c):
        return remote(own(c, g), slot(c, z, g), zsend_l.at[c, 0], zrecv_l.at[c, 1], (g, z - 1, t))

    def right_hop(c, d, src):
        return remote(slot(c, src, g), slot(c, src, g), zsend_r.at[c, d], zrecv_r.at[c, min(d + 1, F - 1)], (g, z + 1, t))

    def left_hop(c, d, src):
        return remote(slot(c, src, g), slot(c, src, g), zsend_l.at[c, d], zrecv_l.at[c, min(d + 1, F - 1)], (g, z - 1, t))

    def arrival(c, d, src, left):
        sems = zrecv_l if left else zrecv_r
        return remote(slot(c, src, g), slot(c, src, g), zsend_r.at[c, d], sems.at[c, d], (g, z, t))

    def across(c, d, src, left):
        return remote(slot(c, src, g), slot(c, src, g), ys[left].at[c, d], yr[left].at[c, d], (other, z, t))

    def across_arrival(c, d, src, left):
        return remote(slot(c, src, other), slot(c, src, other), ys[left].at[c, d], yr[left].at[c, d], (other, z, t))

    issued = [0]

    def own_upto(limit):
        while issued[0] < min(limit, n_chunks):
            c = issued[0]
            issued[0] += 1

            @pl.when(z < F - 1)
            def _():
                own_right(c).start()

            @pl.when(z > 0)
            def _():
                own_left(c).start()

    def both(d, body):
        @pl.when(z - d >= 0)
        def _():
            body(z - d, 0)

        @pl.when(z + d < F)
        def _():
            body(z + d, 1)

    def service(c, d):
        def body(src, left):
            arrival(c, d, src, left).wait_recv()
            if d < F - 1:
                if left:
                    @pl.when(z > 0)
                    def _():
                        left_hop(c, d, src).start()
                else:
                    @pl.when(z < F - 1)
                    def _():
                        right_hop(c, d, src).start()
            across(c, d, src, left).start()

        both(d, body)

    def service_all(c):
        own_upto(c + 1 + AHEAD)
        for d in range(1, F):
            service(c, d)

    def y_wait(c, d):
        both(d, lambda src, left: across_arrival(c, d, src, left).wait_recv())

    def y_wait_all(c):
        for d in range(1, F):
            y_wait(c, d)

    own_upto(1)
    copies = [
        pltpu.make_async_copy(wv, gv.at[pl.ds(mult(z * R, R), R), :], local_sem.at[0]),
        pltpu.make_async_copy(wg, gg.at[pl.ds(mult(z * R, R), R), :], local_sem.at[1]),
        pltpu.make_async_copy(wo, go.at[z], local_sem.at[2]),
        pltpu.make_async_copy(wd, gd.at[z], local_sem.at[3]),
    ]
    for j in range(PIECES):
        copies.append(
            pltpu.make_async_copy(
                wu.at[:, pl.ds(j * HB, HB)], gu.at[j, pl.ds(mult(z * R, R), R), :], local_sem.at[4 + j]
            )
        )
    for copy in copies:
        copy.start()
    own_upto(1 + AHEAD)

    block = 64

    def norm_step(i, carry):
        at = pl.ds(mult(i * block, block), block)
        x = tok[at, :].astype(jnp.float32)
        normed[at, :] = rms_rows(x, norm_in[...].astype(jnp.float32)).astype(jnp.bfloat16)
        return carry

    lax.fori_loop(0, S // block, norm_step, 0)
    for copy in copies:
        copy.wait()

    service_all(0)
    service_all(1)
    own_upto(3 + AHEAD)
    service(2, 1)
    y_wait_all(0)
    y_wait_all(1)

    tile = min(256, C)
    gated[0:PAD, :] = jnp.zeros((PAD, C), jnp.float32)

    def gate_step(i, carry):
        at = pl.ds(mult(i * tile, tile), tile)
        v = jnp.dot(normed[...], gv[:, at], preferred_element_type=jnp.float32)
        a = jnp.dot(normed[...], gg[:, at], preferred_element_type=jnp.float32)
        gated[PAD:, at] = v * jax.nn.sigmoid(a)
        return carry

    lax.fori_loop(0, C // tile, gate_step, 0)

    for d in range(2, F):
        service(2, d)

    span = 128
    lead = PAD - (taps - 1)

    def conv_step(i, carry):
        base = mult(i * span, span)
        first = jnp.zeros((span, 128), jnp.float32)
        second = jnp.zeros((span, 128), jnp.float32)
        for j in range(C // 128):
            lanes = pl.ds(j * 128, 128)
            window = gated[pl.ds(base, span + PAD), lanes]
            weights = conv_k[:, pl.ds(mult(t * C + j * 128, 128), 128)]
            acc = jnp.zeros((span, 128), jnp.float32)
            for k in range(taps):
                acc = acc + weights[k : k + 1, :] * window[lead + k : lead + k + span, :]
            conv[pl.ds(base, span), lanes] = acc
            first = first + acc
            second = second + acc * acc
        lane = lax.broadcasted_iota(jnp.int32, (span, 128), 1)
        both_sums = jnp.where(
            lane == 0,
            jnp.sum(first, axis=1, keepdims=True),
            jnp.where(lane == 1, jnp.sum(second, axis=1, keepdims=True), 0.0),
        )
        st_own[:, pl.ds(base, span)] = jnp.transpose(both_sums)[0:8, :]
        return carry

    lax.fori_loop(0, S // span, conv_step, 0)

    def stat_copy(i):
        return remote(st_own, st_recv.at[i], st_send.at[i], st_rsem.at[i], (g, z, peers[i]))

    for i in range(1, T):
        stat_copy(i).start()
    service_all(3)
    for i in range(1, T):
        stat_copy(i).wait_recv()

    gain = ln_gain[:, pl.ds(mult(t * C, C), C)].astype(jnp.float32)
    shift = ln_shift[:, pl.ds(mult(t * C, C), C)].astype(jnp.float32)

    def act_step(i, carry):
        base = mult(i * span, span)
        at = pl.ds(base, span)
        sums = st_own[:, at]
        for k in range(1, T):
            sums = sums + st_recv[k, :, at]
        mean = sums[0:1, :] / D
        var = sums[1:2, :] / D - mean * mean
        scale = lax.rsqrt(var + 1e-05)
        mean_c = jnp.transpose(jnp.broadcast_to(mean, (128, span)))[:, 0:1]
        scale_c = jnp.transpose(jnp.broadcast_to(scale, (128, span)))[:, 0:1]
        n = (conv[at, :] - mean_c) * scale_c * gain + shift
        act[at, :] = (n * jax.nn.sigmoid(n)).astype(jnp.bfloat16)
        return carry

    lax.fori_loop(0, S // span, act_step, 0)
    y_wait_all(2)

    def out_step(i, carry):
        part[:, pl.ds(mult(i * N, N), N)] = jnp.dot(
            act[...], go[i], preferred_element_type=jnp.float32
        ).astype(jnp.bfloat16)
        return carry

    lax.fori_loop(0, F, out_step, 0)

    def mix_copy(i):
        return remote(
            part.at[pl.ds(mult(peers[i] * rows, rows), rows), :], rs.at[i], rs_send.at[i], rs_rsem.at[i], (g, z, peers[i])
        )

    for i in range(1, T):
        mix_copy(i).start()
    service_all(4)
    service(5, 1)
    for i in range(1, T):
        mix_copy(i).wait_recv()

    small = 32

    def resid_step(i, carry):
        at = pl.ds(mult(i * small, small), small)
        mine = pl.ds(mult(t * rows + i * small, small), small)
        total = part[mine, :].astype(jnp.float32)
        for k in range(1, T):
            total = total + rs[k, at, :].astype(jnp.float32)
        r = tok[mine, :].astype(jnp.float32) + total
        resid[at, :] = r
        nm_own[at, :] = rms_rows(r, norm_mlp[...].astype(jnp.float32)).astype(jnp.bfloat16)
        return carry

    lax.fori_loop(0, rows // small, resid_step, 0)

    def norm_copy(i):
        return remote(
            nm_own, nm.at[pl.ds(mult(t * rows, rows), rows), :], ag_send.at[i], ag_rsem.at[i], (g, z, peers[i])
        )

    def norm_arrival(i):
        return remote(
            nm_own, nm.at[pl.ds(mult(sources[i] * rows, rows), rows), :], ag_send.at[i], ag_rsem.at[i], (g, z, peers[i])
        )

    for i in range(1, T):
        norm_copy(i).start()
    nm[pl.ds(mult(t * rows, rows), rows), :] = nm_own[...]
    own_upto(5 + 1 + AHEAD)
    for d in range(2, F):
        service(5, d)
    service_all(6)
    own_upto(n_chunks)
    for i in range(1, T):
        norm_arrival(i).wait_recv()

    utile = min(256, HB)

    def up_block(j):
        y_wait_all(3 + j)

        def up_step(i, carry):
            at = pl.ds(mult(i * utile, utile), utile)
            a = jnp.dot(nm[...], gu[j, :, at], preferred_element_type=jnp.float32)
            a = jnp.maximum(a, 0.0)
            hidden[:, pl.ds(mult(j * HB + i * utile, utile), utile)] = (a * a).astype(jnp.bfloat16)
            return carry

        lax.fori_loop(0, HB // utile, up_step, 0)

    for j in range(PIECES):
        if j < PIECES - 1:
            up_block(j)
        if F > 1:
            service(first_down + j, 1)
    up_block(PIECES - 1)

    ntile = min(256, N)

    def fin_copy(src, i):
        return remote(
            fin.at[src, pl.ds(mult(peers[i] * rows, rows), rows), :], rs2.at[src, i],
            fs_send.at[src, i], fs_rsem.at[src, i], (g, z, peers[i]),
        )

    def down(src):
        def down_step(i, carry):
            at = pl.ds(mult(i * ntile, ntile), ntile)
            fin[src, :, at] = jnp.dot(
                hidden[...], gd[src, :, at], preferred_element_type=jnp.float32
            ).astype(jnp.bfloat16)
            return carry

        lax.fori_loop(0, N // ntile, down_step, 0)
        for i in range(1, T):
            fin_copy(src, i).start()

    def finish(src):
        for i in range(1, T):
            fin_copy(src, i).wait_recv()
        cols = pl.ds(mult(src * N, N), N)
        total = fin[src, pl.ds(mult(t * rows, rows), rows), :].astype(jnp.float32)
        for k in range(1, T):
            total = total + rs2[src, k].astype(jnp.float32)
        out[:, cols] = (resid[:, cols] + total).astype(jnp.bfloat16)

    down(z)
    for d in range(1, F):
        if d + 1 < F:
            service(first_down, d + 1)
        for c in range(first_down, n_chunks):
            y_wait(c, d)
        both(d, lambda src, left: down(src))
        if d + 1 < F:
            for c in range(first_down + 1, n_chunks):
                service(c, d + 1)
        if d == 1:
            finish(z)
        else:
            both(d - 1, lambda src, left: finish(src))
    both(F - 1, lambda src, left: finish(src))

    for c in range(n_chunks):
        @pl.when(z < F - 1)
        def _():
            own_right(c).wait_send()

        @pl.when(z > 0)
        def _():
            own_left(c).wait_send()

        for d in range(1, F):
            def drain(src, left):
                if d < F - 1:
                    if left:
                        @pl.when(z > 0)
                        def _():
                            left_hop(c, d, src).wait_send()
                    else:
                        @pl.when(z < F - 1)
                        def _():
                            right_hop(c, d, src).wait_send()
                across(c, d, src, left).wait_send()

            both(d, drain)
    for i in range(1, T):
        stat_copy(i).wait_send()
        mix_copy(i).wait_send()
        norm_copy(i).wait_send()
        for src in range(F):
            fin_copy(src, i).wait_send()


def solution(mesh):
    F, T = mesh.shape["fs"], mesh.shape["tp"]

    def step(tokens, norm_in, w_value, w_gate, conv_kernel, ln_gain, ln_shift, w_out, norm_mlp, w_up, w_down):
        S, D = tokens.shape
        R, C = w_value.shape
        H = w_up.shape[1]
        N = w_out.shape[1]
        rows = S // T
        chunks = 3 + 2 * PIECES
        bf16, f32 = jnp.bfloat16, jnp.float32
        dma = pltpu.SemaphoreType.DMA
        vmem = pl.BlockSpec(memory_space=pltpu.VMEM)
        anywhere = pl.BlockSpec(memory_space=pl.ANY)
        return pl.pallas_call(
            functools.partial(kernel, F, T),
            out_shape=jax.ShapeDtypeStruct((rows, D), bf16),
            in_specs=[vmem] * 6 + [anywhere] * 5,
            out_specs=vmem,
            scratch_shapes=[
                pltpu.VMEM((S, D), bf16),
                pltpu.VMEM((D, C), bf16),
                pltpu.VMEM((D, C), bf16),
                pltpu.VMEM((F, C, N), bf16),
                pltpu.VMEM((PIECES, D, H // PIECES), bf16),
                pltpu.VMEM((F, H, N), bf16),
                pltpu.VMEM((S + PAD, C), f32),
                pltpu.VMEM((S, C), f32),
                pltpu.VMEM((S, C), bf16),
                pltpu.VMEM((S, D), bf16),
                pltpu.VMEM((T, rows, D), bf16),
                pltpu.VMEM((rows, D), f32),
                pltpu.VMEM((S, D), bf16),
                pltpu.VMEM((S, H), bf16),
                pltpu.VMEM((F, S, N), bf16),
                pltpu.VMEM((F, T, rows, N), bf16),
                pltpu.VMEM((8, S), f32),
                pltpu.VMEM((T, 8, S), f32),
                pltpu.VMEM((rows, D), bf16),
                dma((4 + PIECES,)),
            ]
            + [dma((chunks, F))] * 8
            + [dma((T,))] * 6
            + [dma((F, T))] * 2,
            compiler_params=pltpu.CompilerParams(
                collective_id=0, has_side_effects=True, vmem_limit_bytes=62 * 1024 * 1024
            ),
        )(
            tokens, norm_in.reshape(1, D), conv_kernel, ln_gain.reshape(1, D), ln_shift.reshape(1, D),
            norm_mlp.reshape(1, D), w_value, w_gate, w_out, w_up, w_down,
        )

    in_specs = (
        P(("grp", "fs"), None), P(), P("fs", "tp"), P("fs", "tp"), P(), P(), P(),
        P("tp", "fs"), P(), P("fs", "tp"), P("tp", "fs"),
    )
    return jax.shard_map(
        step, mesh=mesh, in_specs=in_specs, out_specs=P(("grp", "fs", "tp"), None), check_vma=False
    )
```

time: 560 us -> 237 us (0.42)
  waiting for transfers between devices: 495 us -> 0 us
  Pallas kernels: 0 us -> 229 us
  matrix products: 26.9 us -> 0 us
  other arithmetic: 15 us -> 0 us
  between operations: 13.6 us -> 0.01 us
  blocking collectives: 6.79 us -> 0 us
    all_gather x5 -> x0, waiting for transfers between devices: 413 us -> none  [the longest x1 149 us: shards(): whole_down = lax.all_gather(w_down, 'fs', axis=1, tiled=True)]
    pallas_call x0 -> x1, Pallas kernels: none -> 229 us  [step(): pl.pallas_call(functools.partial(kernel, F, T), out_shape=jax.ShapeDtypeS...]
    psum x1 -> x0, waiting for transfers between devices: 48.9 us -> none  [shards(): lax.psum(partial_value.astype(jnp.bfloat16), 'tp').astype(jnp.float32)]
    reduce_scatter x1 -> x0, waiting for transfers between devices: 29.5 us -> none  [shards(): lax.psum_scatter(jnp.dot(hidden, whole_down, preferred_element_type=jnp.f...]
    dot_general x4 -> x0, matrix products: 26.9 us -> none  [the longest x1 16.6 us: shards(): jnp.dot(hidden, whole_down, preferred_element_type=jnp.float32)]
    reduce_sum x2 -> x0, other arithmetic: 7.04 us -> none  [the longest x1 4.97 us: shards(): jnp.sum(convolved, axis=1)]
    psum x1 -> x0, blocking collectives: 6.79 us -> none  [shards(): lax.psum((jnp.sum(convolved, axis=1), jnp.sum(convolved * convolved, axis...]
  transfers between devices with their start and end apart: 7 -> 0, of which waited for: 7 -> 0; matrix products, arithmetic and copies ran while one was open for 4% -> 0% of each run, Pallas kernels for 0% -> 0%
where the time goes in v1:
time: 237 us; the launch traced here: 236 us
  Pallas kernels  229 us (97%)
  local copies, waits for them, and re-layouts  7.03 us (3%)
    pallas_call x1, Pallas kernels, step(): pl.pallas_call(functools.partial(kernel, F, T), out_shape=jax.ShapeDtypeS...  229 us

profile of v1, /device:TPU:0, one launch (start us, length us, event | category | flops | bytes accessed | tf_op | source)
XLA Modules:
  0.0 236.2 jit_solution(1103529212437259247)
XLA Ops:
  0.0 1.3 reshape.12.norm_in
  1.3 1.3 reshape.13.ln_gain
  2.6 1.3 reshape.14.ln_shift
  3.9 1.3 reshape.15.norm_mlp
  5.1 229.2 %shard_map.109 = bf16[128,2048]{1,0:T(8,128)(2,1)} custom-call(bf16[512,2048]{1,0:T(8,128)(2,1)} %tok.1, bf16[1,2048]{1,0:T(2,128)(2,1)} %reshape.12.norm_in, f32[31,2048]{1,0:T(8,128)} %conv_k.1, bf16[1,2048]{1,0:T(2,128)(2,1)} %reshape.13.ln_gain, bf16[1,2048]{1,0:T(2,128)(2,1)} %reshape.14.ln_shift, bf16[1,2048]{1,0:T(2,128)(2,1)} %reshape.15.norm_mlp, ...), custom_call_target="tpu_custom_call" | custom-call | tf_op jit(solution)/shard_map/pallas_call | solution.py:445
  234.3 1.9 copy.13

commit v2 on v1

--- a/solution.py
+++ b/solution.py
@@ -22,9 +22,11 @@
     tok, norm_in, conv_k, ln_gain, ln_shift, norm_mlp, wv, wg, wo, wu, wd,
     out,
     normed, gv, gg, go, gu, gd, gated, conv, act, part, rs, resid, nm, hidden, fin, rs2,
+    nm_e, hid_e, fin_e, rs_e, sum_e, ret,
     st_own, st_recv, nm_own,
     local_sem, zsend_r, zsend_l, zrecv_r, zrecv_l, ysend_r, ysend_l, yrecv_r, yrecv_l,
     st_send, st_rsem, rs_send, rs_rsem, ag_send, ag_rsem, fs_send, fs_rsem,
+    rest, ex_sem, ea_send, ea_rsem, fe_send, fe_rsem, ret_send, ret_rsem,
 ):
     g = lax.axis_index("grp")
     z = lax.axis_index("fs")
@@ -41,6 +43,39 @@
     n_chunks = 3 + 2 * PIECES
     first_down = 3 + PIECES
 
+    LOW = PIECES // 2
+    HL = LOW * HB
+    at_left, at_right = z == 0, z == F - 1
+    is_end = jnp.logical_or(at_left, at_right)
+    help_left, help_right = z == 1, z == F - 2
+
+    def upper(c):
+        return c >= 3 and (c - 3) % PIECES >= LOW
+
+    def when_right(c):
+        return pl.when(z < F - 1 - upper(c))
+
+    def when_left(c):
+        return pl.when(z > 0 + upper(c))
+
+    def for_ends(body):
+        @pl.when(at_left)
+        def _():
+            body(z + 1)
+
+        @pl.when(at_right)
+        def _():
+            body(z - 1)
+
+    def for_helpers(body):
+        @pl.when(help_left)
+        def _():
+            body(z - 1)
+
+        @pl.when(help_right)
+        def _():
+            body(z + 1)
+
     def mult(i, k):
         return pl.multiple_of(i, k)
 
@@ -50,7 +85,7 @@
             return ref.at[pl.ds(mult(h * size, size), size), :]
         if c < first_down:
             return wu.at[pl.ds(mult(h * R2, R2), R2), pl.ds((c - 3) * HB, HB)]
-        return wd.at[pl.ds(mult(h * H2 + (c - first_down) * HC, HC), HC), :]
+        return wd.at[pl.ds(mult((c - first_down) * HB + h * HC, HC), HC), :]
 
     def slot(c, src, h):
         if c < 2:
@@ -59,7 +94,7 @@
             return go.at[src, pl.ds(mult(h * C2, C2), C2), :]
         if c < first_down:
             return gu.at[c - 3, pl.ds(mult(src * R + h * R2, R2), R2), :]
-        return gd.at[src, pl.ds(mult(h * H2 + (c - first_down) * HC, HC), HC), :]
+        return gd.at[src, pl.ds(mult((c - first_down) * HB + h * HC, HC), HC), :]
 
     def remote(src_ref, dst_ref, send, recv, device):
         return pltpu.make_async_remote_copy(
@@ -114,6 +149,9 @@
     def across_arrival(c, d, src, left):
         return remote(slot(c, src, other), slot(c, src, other), ys[left].at[c, d], yr[left].at[c, d], (other, z, t))
 
+    def own_rest(c, helper):
+        return remote(own(c, other), slot(c, z, other), ex_sem.at[2 + c], rest.at[c], (g, helper, t))
+
     issued = [0]
 
     def own_upto(limit):
@@ -121,38 +159,51 @@
             c = issued[0]
             issued[0] += 1
 
-            @pl.when(z < F - 1)
+            @when_right(c)
             def _():
                 own_right(c).start()
 
-            @pl.when(z > 0)
+            @when_left(c)
             def _():
                 own_left(c).start()
 
-    def both(d, body):
-        @pl.when(z - d >= 0)
+            for_ends(lambda helper: own_rest(c, helper).start())
+
+    def both(d, body, c=0):
+        @pl.when(jnp.logical_and(z - d >= 0, z < F - upper(c)))
         def _():
             body(z - d, 0)
 
-        @pl.when(z + d < F)
+        @pl.when(jnp.logical_and(z + d < F, z >= 0 + upper(c)))
         def _():
             body(z + d, 1)
+
+    def when_across(d, left):
+        if d > 1:
+            return lambda body: body()
+        return pl.when(z != (F - 2 if left else 1))
+
+    def forward(c, d, src, left, act_on):
+        if d < F - 1:
+            if left:
+                @when_left(c)
+                def _():
+                    act_on(left_hop(c, d, src))
+            else:
+                @when_right(c)
+                def _():
+                    act_on(right_hop(c, d, src))
+
+        @when_across(d, left)
+        def _():
+            act_on(across(c, d, src, left))
 
     def service(c, d):
         def body(src, left):
             arrival(c, d, src, left).wait_recv()
-            if d < F - 1:
-                if left:
-                    @pl.when(z > 0)
-                    def _():
-                        left_hop(c, d, src).start()
-                else:
-                    @pl.when(z < F - 1)
-                    def _():
-                        right_hop(c, d, src).start()
-            across(c, d, src, left).start()
-
-        both(d, body)
+            forward(c, d, src, left, lambda copy: copy.start())
+
+        both(d, body, c)
 
     def service_all(c):
         own_upto(c + 1 + AHEAD)
@@ -160,7 +211,17 @@
             service(c, d)
 
     def y_wait(c, d):
-        both(d, lambda src, left: across_arrival(c, d, src, left).wait_recv())
+        def body(src, left):
+            @when_across(d, left)
+            def _():
+                across_arrival(c, d, src, left).wait_recv()
+
+            if d == 1:
+                @pl.when(z == (F - 2 if left else 1))
+                def _():
+                    remote(slot(c, src, other), slot(c, src, other), ex_sem.at[0], rest.at[c], (g, src, t)).wait_recv()
+
+        both(d, body, c)
 
     def y_wait_all(c):
         for d in range(1, F):
@@ -322,12 +383,32 @@
 
     for i in range(1, T):
         norm_copy(i).start()
-    nm[pl.ds(mult(t * rows, rows), rows), :] = nm_own[...]
+    mine = pl.ds(mult(t * rows, rows), rows)
+
+    def give_copy(helper):
+        return remote(nm_own, nm_e.at[mine, :], ex_sem.at[0], ex_sem.at[1], (g, helper, t))
+
+    for_ends(lambda helper: give_copy(helper).start())
+    nm[mine, :] = nm_own[...]
     own_upto(5 + 1 + AHEAD)
     for d in range(2, F):
         service(5, d)
     service_all(6)
     own_upto(n_chunks)
+
+    def share_copy(i):
+        return remote(nm_e.at[mine, :], nm_e.at[mine, :], ea_send.at[i], ea_rsem.at[i], (g, z, peers[i]))
+
+    def share_arrival(i):
+        there = pl.ds(mult(sources[i] * rows, rows), rows)
+        return remote(nm_e.at[there, :], nm_e.at[there, :], ea_send.at[i], ea_rsem.at[i], (g, z, peers[i]))
+
+    def share(end):
+        remote(nm_own, nm_e.at[mine, :], ex_sem.at[0], ex_sem.at[1], (g, end, t)).wait_recv()
+        for i in range(1, T):
+            share_copy(i).start()
+
+    for_helpers(share)
     for i in range(1, T):
         norm_arrival(i).wait_recv()
 
@@ -345,12 +426,35 @@
 
         lax.fori_loop(0, HB // utile, up_step, 0)
 
+    def up_some(j):
+        if j < LOW:
+            up_block(j)
+        else:
+            @pl.when(jnp.logical_not(is_end))
+            def _():
+                up_block(j)
+
     for j in range(PIECES):
         if j < PIECES - 1:
-            up_block(j)
-        if F > 1:
-            service(first_down + j, 1)
-    up_block(PIECES - 1)
+            up_some(j)
+        service(first_down + j, 1)
+    up_some(PIECES - 1)
+
+    def up_for_end(end):
+        for i in range(1, T):
+            share_arrival(i).wait_recv()
+        per = HB // utile
+
+        def up_step(i, carry):
+            at = pl.ds(mult(lax.rem(i, per) * utile, utile), utile)
+            a = jnp.dot(nm_e[...], gu[LOW + lax.div(i, per), :, at], preferred_element_type=jnp.float32)
+            a = jnp.maximum(a, 0.0)
+            hid_e[:, pl.ds(mult(i * utile, utile), utile)] = (a * a).astype(jnp.bfloat16)
+            return carry
+
+        lax.fori_loop(0, (PIECES - LOW) * per, up_step, 0)
+
+    for_helpers(up_for_end)
 
     ntile = min(256, N)
 
@@ -360,15 +464,60 @@
             fs_send.at[src, i], fs_rsem.at[src, i], (g, z, peers[i]),
         )
 
-    def down(src):
+    def end_copy(src, i):
+        return remote(
+            fin_e.at[src, pl.ds(mult(peers[i] * rows, rows), rows), :], rs_e.at[src, i],
+            fe_send.at[src, i], fe_rsem.at[src, i], (g, z, peers[i]),
+        )
+
+    def down_for_end(src):
         def down_step(i, carry):
             at = pl.ds(mult(i * ntile, ntile), ntile)
-            fin[src, :, at] = jnp.dot(
-                hidden[...], gd[src, :, at], preferred_element_type=jnp.float32
+            fin_e[src, :, at] = jnp.dot(
+                hid_e[...], gd[src, HL:, at], preferred_element_type=jnp.float32
             ).astype(jnp.bfloat16)
             return carry
 
         lax.fori_loop(0, N // ntile, down_step, 0)
+        for i in range(1, T):
+            end_copy(src, i).start()
+
+    def ret_copy(src, end):
+        return remote(sum_e.at[src], ret.at[src], ret_send.at[src], ret_rsem.at[src], (g, end, t))
+
+    def return_sum(src):
+        def body(end):
+            for i in range(1, T):
+                end_copy(src, i).wait_recv()
+            total = fin_e[src, mine, :].astype(jnp.float32)
+            for k in range(1, T):
+                total = total + rs_e[src, k].astype(jnp.float32)
+            sum_e[src] = total.astype(jnp.bfloat16)
+            ret_copy(src, end).start()
+
+        for_helpers(body)
+
+    def down(src):
+        for_helpers(lambda end: down_for_end(src))
+
+        def rows_to(limit):
+            def down_step(i, carry):
+                at = pl.ds(mult(i * ntile, ntile), ntile)
+                fin[src, :, at] = jnp.dot(
+                    hidden[:, :limit], gd[src, :limit, at], preferred_element_type=jnp.float32
+                ).astype(jnp.bfloat16)
+                return carry
+
+            lax.fori_loop(0, N // ntile, down_step, 0)
+
+        @pl.when(is_end)
+        def _():
+            rows_to(HL)
+
+        @pl.when(jnp.logical_not(is_end))
+        def _():
+            rows_to(H)
+
         for i in range(1, T):
             fin_copy(src, i).start()
 
@@ -376,10 +525,10 @@
         for i in range(1, T):
             fin_copy(src, i).wait_recv()
         cols = pl.ds(mult(src * N, N), N)
-        total = fin[src, pl.ds(mult(t * rows, rows), rows), :].astype(jnp.float32)
+        total = fin[src, mine, :].astype(jnp.float32)
         for k in range(1, T):
             total = total + rs2[src, k].astype(jnp.float32)
-        out[:, cols] = (resid[:, cols] + total).astype(jnp.bfloat16)
+        resid[:, cols] = resid[:, cols] + total
 
     down(z)
     for d in range(1, F):
@@ -392,34 +541,51 @@
             for c in range(first_down + 1, n_chunks):
                 service(c, d + 1)
         if d == 1:
-            finish(z)
+            return_sum(z)
         else:
-            both(d - 1, lambda src, left: finish(src))
-    both(F - 1, lambda src, left: finish(src))
+            both(d - 1, lambda src, left: return_sum(src))
+    both(F - 1, lambda src, left: return_sum(src))
+
+    def finish_step(src, carry):
+        finish(src)
+
+        def add(helper):
+            cols = pl.ds(mult(src * N, N), N)
+            ret_copy(src, helper).wait_recv()
+            resid[:, cols] = resid[:, cols] + ret[src].astype(jnp.float32)
+
+        for_ends(add)
+        cols = pl.ds(mult(src * N, N), N)
+        out[:, cols] = resid[:, cols].astype(jnp.bfloat16)
+        return carry
+
+    lax.fori_loop(0, F, finish_step, 0)
 
     for c in range(n_chunks):
-        @pl.when(z < F - 1)
+        @when_right(c)
         def _():
             own_right(c).wait_send()
 
-        @pl.when(z > 0)
+        @when_left(c)
         def _():
             own_left(c).wait_send()
 
+        for_ends(lambda helper: own_rest(c, helper).wait_send())
+
         for d in range(1, F):
-            def drain(src, left):
-                if d < F - 1:
-                    if left:
-                        @pl.when(z > 0)
-                        def _():
-                            left_hop(c, d, src).wait_send()
-                    else:
-                        @pl.when(z < F - 1)
-                        def _():
-                            right_hop(c, d, src).wait_send()
-                across(c, d, src, left).wait_send()
-
-            both(d, drain)
+            both(d, lambda src, left: forward(c, d, src, left, lambda copy: copy.wait_send()), c)
+
+    for_ends(lambda helper: give_copy(helper).wait_send())
+
+    def drain_helper(end):
+        for i in range(1, T):
+            share_copy(i).wait_send()
+            for src in range(F):
+                end_copy(src, i).wait_send()
+        for src in range(F):
+            ret_copy(src, end).wait_send()
+
+    for_helpers(drain_helper)
     for i in range(1, T):
         stat_copy(i).wait_send()
         mix_copy(i).wait_send()
@@ -464,6 +630,12 @@
                 pltpu.VMEM((S, H), bf16),
                 pltpu.VMEM((F, S, N), bf16),
                 pltpu.VMEM((F, T, rows, N), bf16),
+                pltpu.VMEM((S, D), bf16),
+                pltpu.VMEM((S, H - H // PIECES * (PIECES // 2)), bf16),
+                pltpu.VMEM((F, S, N), bf16),
+                pltpu.VMEM((F, T, rows, N), bf16),
+                pltpu.VMEM((F, rows, N), bf16),
+                pltpu.VMEM((F, rows, N), bf16),
                 pltpu.VMEM((8, S), f32),
                 pltpu.VMEM((T, 8, S), f32),
                 pltpu.VMEM((rows, D), bf16),
@@ -471,7 +643,10 @@
             ]
             + [dma((chunks, F))] * 8
             + [dma((T,))] * 6
-            + [dma((F, T))] * 2,
+            + [dma((F, T))] * 2
+            + [dma((chunks,)), dma((2 + chunks,)), dma((T,)), dma((T,))]
+            + [dma((F, T))] * 2
+            + [dma((F,))] * 2,
             compiler_params=pltpu.CompilerParams(
                 collective_id=0, has_side_effects=True, vmem_limit_bytes=62 * 1024 * 1024
             ),

time: 237 us -> 206 us (0.87)
  Pallas kernels: 229 us -> 199 us
    pallas_call x1, Pallas kernels: 229 us -> 199 us  [step(): pl.pallas_call(functools.partial(kernel, F, T), out_shape=jax.ShapeDtypeS...]
where the time goes in v2:
time: 206 us
  Pallas kernels  199 us (97%)
  local copies, waits for them, and re-layouts  7.03 us (3%)
    pallas_call x1, Pallas kernels, step(): pl.pallas_call(functools.partial(kernel, F, T), out_shape=jax.ShapeDtypeS...  199 us

profile of v2, /device:TPU:0, one launch (start us, length us, event | category | flops | bytes accessed | tf_op | source)
XLA Modules:
  0.0 206.1 jit_solution(6798131199136912077)
XLA Ops:
  0.0 1.3 reshape.12.norm_in
  1.3 1.3 reshape.13.ln_gain
  2.6 1.3 reshape.14.ln_shift
  3.9 1.3 reshape.15.norm_mlp
  5.1 199.1 %shard_map.109 = bf16[128,2048]{1,0:T(8,128)(2,1)} custom-call(bf16[512,2048]{1,0:T(8,128)(2,1)} %tok.1, bf16[1,2048]{1,0:T(2,128)(2,1)} %reshape.12.norm_in, f32[31,2048]{1,0:T(8,128)} %conv_k.1, bf16[1,2048]{1,0:T(2,128)(2,1)} %reshape.13.ln_gain, bf16[1,2048]{1,0:T(2,128)(2,1)} %reshape.14.ln_shift, bf16[1,2048]{1,0:T(2,128)(2,1)} %reshape.15.norm_mlp, ...), custom_call_target="tpu_custom_call" | custom-call | tf_op jit(solution)/shard_map/pallas_call | solution.py:611
  204.2 1.9 copy.13
